TPU v7x, 32 devices: a whole 2x2x4 slice. The times are simulated.
32 devices in a mesh: sp: 8 (over z, x), tp: 4 (over y, core).
Axes of the slice: x: 2, y: 2, z: 4, core: 2. Of those that a mesh axis runs over, the one named last changes fastest.
Arguments:
- tokens: bfloat16 [8192, 2048], P('sp'), may hold values from -6 to 6
- pre_gain: float32 [2048], replicated, may hold values from 0.1 to 1.9
- w_query: bfloat16 [2048, 2048], P(None, 'tp'), may hold values from -0.125 to 0.125
- w_key: bfloat16 [2048, 2048], P(None, 'tp'), may hold values from -0.125 to 0.125
- w_value: bfloat16 [2048, 2048], P(None, 'tp'), may hold values from -0.125 to 0.125
- memory_output_gate_weight: bfloat16 [2048, 2048], P(None, 'tp'), may hold values from -0.125 to 0.125
- w_input_gate: bfloat16 [2048, 8], replicated, may hold values from -0.125 to 0.125
- w_forget_gate: bfloat16 [2048, 8], replicated, may hold values from -0.125 to 0.125
- input_bias: float32 [8], replicated, may hold values from -3 to 220
- forget_bias: float32 [8], replicated, may hold values from 3.9 to 12.4
- forget_extra: float32 [8192, 8], P('sp', 'tp'), may hold values from -1.5 to 0
- initial_memory: float32 [8, 256, 256], P('tp', 'sp'), may hold values from -2048 to 2048
- initial_normal: float32 [8, 256], P('tp', 'sp'), may hold values from -2048 to 2048
- memory_gain: float32 [2048], replicated, may hold values from 0.1 to 1.9
- w_pool_input: bfloat16 [2048, 1024], P(None, 'tp'), may hold values from -0.125 to 0.125
- w_pool_gate: bfloat16 [2048, 1024], P(None, 'tp'), may hold values from -0.125 to 0.125
- pool_mix: bfloat16 [8, 128, 128], replicated, may hold values from -0.5 to 0.5
- pool_gain: float32 [1024], replicated, may hold values from 0.1 to 1.9
- w_out_memory: bfloat16 [2048, 2048], P('tp'), may hold values from -0.109375 to 0.109375
- w_out_pool: bfloat16 [1024, 2048], P('tp'), may hold values from -0.109375 to 0.109375
- post_gain: float32 [2048], replicated, may hold values from 0.1 to 1.9
Outputs:
- layer_out: bfloat16 [8192, 2048], P(('sp', 'tp'))
All inputs are finite; a program needn't handle non-finite values.
Results may differ from a plain program's by a relative error of at most 0.018.
The roundings to bfloat16 on the way count: a program that leaves them out, or rounds other values in their place, can miss the bound.
Values may be sent and summed in bfloat16 or wider, within the bound.
A program may use at most 128 MiB of HBM per device.

v0:
```python
import jax
import jax.numpy as jnp
from jax import lax
from jax.sharding import PartitionSpec as P

HEAD_DIM = 256
MEM_WIDTH = 2048
GROUP_DIM = 128
WIDEST = 256
BLOCK = 512


EPS = 1e-06
FLOOR = -1e30


def prefix_2(value, axis, join, neutral):
    count, mine = (lax.axis_size(axis), lax.axis_index(axis))
    pieces = jax.tree.map(lambda part: lax.all_gather(part, axis), value)
    total = jax.tree.map(
        lambda part, zero: jnp.full_like(part, 0) + jnp.asarray(zero, part.dtype), value, neutral
    )

    def lap(position, total):
        longer = join(total, jax.tree.map(lambda part: part[position], pieces))
        return jax.tree.map(lambda new, old: jnp.where(position < mine, new, old), longer, total)

    return lax.fori_loop(0, count - 1, lap, total)


def passed_along(value, axis, steps):
    count = lax.axis_size(axis)
    first, last = (max(0, -steps), min(count, count - steps))
    return lax.ppermute(value, axis, [(source, source + steps) for source in range(first, last)])


def normalize(values, gain):
    return values * lax.rsqrt(jnp.mean(values * values, axis=-1, keepdims=True) + EPS) * gain


def block_parts(memory_carry, block_inputs):
    matrix_memory_state, memory_normal, stabilizer = memory_carry
    queries, keys_in, incoming_values, log_input, log_keep = block_inputs
    length = queries.shape[1]
    head_scale = queries.shape[2] ** (-0.5)
    causal = jnp.arange(length)[:, None] >= jnp.arange(length)[None, :]
    running_keep = jnp.cumsum(log_keep, axis=-1)
    decayed = jnp.where(
        causal[None],
        running_keep[:, :, None] - running_keep[:, None, :] + log_input[:, None, :],
        -jnp.inf,
    )
    carried = running_keep + stabilizer[:, None]
    row_max = jnp.maximum(jnp.max(decayed, axis=-1), carried)
    wide_queries = queries.astype(jnp.float32)
    scores = jnp.einsum("hld,hsd->hls", queries, keys_in, preferred_element_type=jnp.float32)
    weights = jnp.exp(decayed - row_max[:, :, None]) * scores * head_scale
    carry_weight = jnp.exp(carried - row_max) * head_scale
    numerator = jnp.einsum(
        "hls,hsd->hld",
        weights.astype(jnp.bfloat16),
        incoming_values,
        preferred_element_type=jnp.float32,
    )
    numerator = numerator + carry_weight[:, :, None] * jnp.einsum(
        "hld,hde->hle", wide_queries, matrix_memory_state, precision=lax.Precision.HIGHEST
    )
    denominator = jnp.sum(weights, axis=-1) + carry_weight * jnp.einsum(
        "hld,hd->hl", wide_queries, memory_normal, precision=lax.Precision.HIGHEST
    )
    block_keep = running_keep[:, -1]
    write_log = block_keep[:, None] - running_keep + log_input
    new_stabilizer = jnp.maximum(block_keep + stabilizer, jnp.max(write_log, axis=-1))
    decay_factor = jnp.exp(block_keep + stabilizer - new_stabilizer)
    write_weight = jnp.exp(write_log - new_stabilizer[:, None])
    key_projected = write_weight[:, :, None] * keys_in.astype(jnp.float32)
    matrix_memory_state = decay_factor[:, None, None] * matrix_memory_state + jnp.einsum(
        "gbq,gbd->gqd",
        key_projected.astype(jnp.bfloat16),
        incoming_values,
        preferred_element_type=jnp.float32,
    )
    memory_normal = decay_factor[:, None] * memory_normal + jnp.sum(key_projected, axis=1)
    return ((matrix_memory_state, memory_normal, new_stabilizer), (numerator, denominator, row_max))


def chain_combine(earlier, later):
    early_state, early_normal, early_stab, early_keep = earlier
    late_state, late_normal, late_stab, late_keep = later
    joint = jnp.maximum(late_stab, late_keep + early_stab)
    late_factor = jnp.exp(late_stab - joint)
    early_factor = jnp.exp(late_keep + early_stab - joint)
    merged_state = (
        late_state * late_factor[:, None, None] + early_state * early_factor[:, None, None]
    )
    merged_normal = late_normal * late_factor[:, None] + early_normal * early_factor[:, None]
    return (merged_state, merged_normal, joint, early_keep + late_keep)


def body(
    tokens,
    pre_gain,
    w_query,
    w_key,
    w_value,
    memory_output_gate_weight,
    w_input_gate,
    w_forget_gate,
    input_bias,
    forget_bias,
    forget_extra,
    initial_memory,
    initial_normal,
    memory_gain,
    w_pool_input,
    w_pool_gate,
    pool_mix,
    pool_gain,
    w_out_memory,
    w_out_pool,
    post_gain,
):
    token_count = tokens.shape[0]
    local_heads = w_query.shape[1] // HEAD_DIM
    local_groups = w_pool_input.shape[1] // GROUP_DIM
    head_index = lax.axis_index("tp")
    first_head = head_index * local_heads
    first_group = head_index * local_groups
    normed = normalize(tokens.astype(jnp.float32), pre_gain).astype(jnp.bfloat16)

    def by_heads(weight):
        shaped = weight.reshape(weight.shape[0], local_heads, HEAD_DIM)
        return jnp.einsum("td,dhe->hte", normed, shaped, preferred_element_type=jnp.float32)

    queries = by_heads(w_query).astype(jnp.bfloat16)
    keys_all = by_heads(w_key).astype(jnp.bfloat16)
    values_all = by_heads(w_value).astype(jnp.bfloat16)
    memory_gate = by_heads(memory_output_gate_weight)
    input_cols = lax.dynamic_slice_in_dim(w_input_gate, first_head, local_heads, 1)
    forget_cols = lax.dynamic_slice_in_dim(w_forget_gate, first_head, local_heads, 1)
    input_shift = lax.dynamic_slice_in_dim(input_bias, first_head, local_heads, 0)
    forget_shift = lax.dynamic_slice_in_dim(forget_bias, first_head, local_heads, 0)
    log_input = (jnp.dot(normed, input_cols, preferred_element_type=jnp.float32) + input_shift).T
    log_keep = (
        jax.nn.log_sigmoid(
            jnp.dot(normed, forget_cols, preferred_element_type=jnp.float32) + forget_shift
        )
        + forget_extra
    ).T
    block_total = token_count // BLOCK

    def split(array):
        return jnp.moveaxis(
            array.reshape((local_heads, block_total, BLOCK) + array.shape[2:]), 1, 0
        )

    def join(array):
        return jnp.moveaxis(array, 0, 1).reshape((local_heads, token_count) + array.shape[3:])

    empty_state = jnp.zeros((local_heads, HEAD_DIM, HEAD_DIM), jnp.float32)
    empty_normal = jnp.zeros((local_heads, HEAD_DIM), jnp.float32)
    empty_stab = jnp.full((local_heads,), FLOOR, jnp.float32)
    summary, (numerator, denominator, row_max) = lax.scan(
        block_parts,
        (empty_state, empty_normal, empty_stab),
        (split(queries), split(keys_all), split(values_all), split(log_input), split(log_keep)),
    )
    summary_state, summary_normal, summary_stab = summary
    numerator, denominator, row_max = (join(numerator), join(denominator), join(row_max))
    keep_total = jnp.sum(log_keep, axis=1)
    keep_running = jnp.cumsum(log_keep, axis=1)
    start_memory, start_normal = (
        lax.all_gather(initial_memory, "sp", axis=1, tiled=True),
        lax.all_gather(initial_normal, "sp", axis=1, tiled=True),
    )
    identity = (empty_state, empty_normal, empty_stab, jnp.zeros((local_heads,), jnp.float32))
    prefix = prefix_2(
        (summary_state, summary_normal, summary_stab, keep_total), "sp", chain_combine, identity
    )
    zero_heads = jnp.zeros((local_heads,), jnp.float32)
    enter_state, enter_normal, enter_stab, _ = chain_combine(
        (start_memory, start_normal, zero_heads, zero_heads), prefix
    )
    head_scale = HEAD_DIM ** (-0.5)
    carried = keep_running + enter_stab[:, None]
    joint_max = jnp.maximum(row_max, carried)
    local_weight = jnp.exp(row_max - joint_max)
    carry_weight = jnp.exp(carried - joint_max) * head_scale
    wide_queries = queries.astype(jnp.float32)
    numerator = numerator * local_weight[:, :, None] + carry_weight[:, :, None] * jnp.einsum(
        "hld,hde->hle", wide_queries, enter_state, precision=lax.Precision.HIGHEST
    )
    denominator = denominator * local_weight + carry_weight * jnp.einsum(
        "hld,hd->hl", wide_queries, enter_normal, precision=lax.Precision.HIGHEST
    )
    memory_rows = numerator / jnp.maximum(jnp.abs(denominator), jnp.exp(-joint_max))[:, :, None]
    local_squares = jnp.sum(memory_rows * memory_rows, axis=(0, 2))
    all_squares = lax.psum(local_squares, "tp")
    row_scale = lax.rsqrt(all_squares / MEM_WIDTH + EPS)
    gain_local = lax.dynamic_slice_in_dim(
        memory_gain, first_head * HEAD_DIM, local_heads * HEAD_DIM, 0
    ).reshape(local_heads, 1, HEAD_DIM)
    memory_out = (
        memory_rows * row_scale[None, :, None] * gain_local * jax.nn.silu(memory_gate)
    ).astype(jnp.bfloat16)
    pool_input = jnp.dot(normed, w_pool_input, preferred_element_type=jnp.float32).astype(
        jnp.bfloat16
    )
    rim_rows = passed_along(pool_input[token_count - WIDEST :], "sp", 1)
    extended = jnp.concatenate([rim_rows, pool_input], axis=0)
    group_ids = first_group + jnp.arange(local_groups)
    windows = jnp.left_shift(2, group_ids)
    target_rows = jnp.arange(token_count)[:, None]
    source_rows = jnp.arange(token_count + WIDEST)[None, :] - WIDEST
    inside = (source_rows <= target_rows)[None] & (
        source_rows[None] > target_rows[None] - windows[:, None, None]
    )
    band = inside.astype(jnp.bfloat16)
    window_sums = jnp.einsum(
        "gts,sgc->tgc",
        band,
        extended.reshape(token_count + WIDEST, local_groups, GROUP_DIM),
        preferred_element_type=jnp.float32,
    )
    global_rows = lax.axis_index("sp") * token_count + jnp.arange(token_count)
    counts = jnp.minimum(global_rows[:, None] + 1, windows[None, :]).astype(jnp.float32)
    grouped = pool_input.astype(jnp.float32).reshape(token_count, local_groups, GROUP_DIM)
    pooled = (window_sums / counts[:, :, None] - grouped).astype(jnp.bfloat16)
    mix_local = lax.dynamic_slice_in_dim(pool_mix, first_group, local_groups, 0)
    mixed = jnp.einsum("tgc,gce->tge", pooled, mix_local, preferred_element_type=jnp.float32)
    pool_gate = jnp.dot(normed, w_pool_gate, preferred_element_type=jnp.float32)
    pool_scale = lax.dynamic_slice_in_dim(
        pool_gain, first_group * GROUP_DIM, local_groups * GROUP_DIM, 0
    )
    pool_out = (
        mixed.reshape(token_count, local_groups * GROUP_DIM) * pool_scale * jax.nn.silu(pool_gate)
    ).astype(jnp.bfloat16)
    out_memory = w_out_memory.reshape(local_heads, HEAD_DIM, w_out_memory.shape[1])
    memory_term = jnp.einsum(
        "hte,hed->td", memory_out, out_memory, preferred_element_type=jnp.float32
    )
    summed = lax.psum_scatter(
        (memory_term + jnp.dot(pool_out, w_out_pool, preferred_element_type=jnp.float32)).astype(
            jnp.bfloat16
        ),
        "tp",
        scatter_dimension=0,
        tiled=True,
    ).astype(jnp.float32)
    return normalize(summed, post_gain).astype(jnp.bfloat16)


def solution(mesh):
    in_specs = (
        P("sp", None),
        P(),
        P(None, "tp"),
        P(None, "tp"),
        P(None, "tp"),
        P(None, "tp"),
        P(),
        P(),
        P(),
        P(),
        P("sp", "tp"),
        P("tp", "sp", None),
        P("tp", "sp"),
        P(),
        P(None, "tp"),
        P(None, "tp"),
        P(),
        P(),
        P("tp", None),
        P("tp", None),
        P(),
    )
    out_specs = P(("sp", "tp"), None)
    return jax.shard_map(body, mesh=mesh, in_specs=in_specs, out_specs=out_specs, check_vma=False)
```

profile of v0, /device:TPU:10, one launch (start us, length us, event | category | flops | bytes accessed | tf_op | source)
XLA Modules:
  0.0 282.7 jit_solution(17413228400965669133)
XLA Ops:
  8.2 3.2 %fusion.48 = f32[1024]{0:T(1024)S(1)} fusion(bf16[1024,2048]{1,0:T(8,128)(2,1)} %param.25), kind=kLoop, calls=%fused_computation.82 | loop fusion | flops 6290432 | bytes 4198400 | tf_op jit(solution)/shard_map/reduce_sum | solution.py:38
  13.2 2.3 fusion.89
  15.7 2.3 fusion.84
  18.1 2.3 fusion.79
  21.5 1.9 convolution_add_fusion.1
  23.4 1.5 copy_bitcast_fusion.1
  25.0 2.1 fusion.147
  27.1 21.6 %while.41 = (s32[]{:T(128)}, f32[2,256,256]{2,1,0:T(8,128)S(1)}, f32[2,256]{1,0:T(2,128)S(1)}, f32[2]{0:T(128)S(1)}, f32[2,2,512,256]{3,2,1,0:T(8,128)}, /*index...) while((s32[]{:T(128)}, f32[2,256,256]{2,1,0:T(8,128)S(1)}, ...), condition=%wide.region_8.9_spmd.clone, body=%wide.region_1.8_spmd.clone.sunk | while | flops 1488860160 | bytes 41355404 | solution.py:163
  30.2 1.5 fusion.197
  32.4 2.3 fusion.195
  40.9 1.5 fusion.197
  43.1 2.3 fusion.195
  49.6 3.8 %convolution_convert_fusion = bf16[1024,256]{0,1:T(8,128)(2,1)S(1)} fusion(bf16[1024,2048]{1,0:T(8,128)(2,1)} %copy-done.1, bf16[2048,256]{1,0:T(8,128)(2,1)} %param.39), kind=kOutput, calls=%fused_computation.125 | convolution fusion | flops 1074003968 | bytes 5767168 | tf_op jit(solution)/shard_map/dot_general | solution.py:206
  55.0 3.4 %collective-permute-start = (bf16[256,256]{0,1:T(8,128)(2,1)S(1)}, bf16[256,256]{0,1:T(8,128)(2,1)S(1)}, u32[]{:S(2)}, u32[]{:S(2)}) collective-permute-start(bf16[256,256]{0,1:T(8,128)(2,1)S(1)} %slice.27), channel_id=1, source_target_pairs={{0,4},{4,8},{8,12},{12,16},{16,20},{20,24},{24,28},{1,5},{5,9},{9,... | collective-permute-start | bytes 393224 | tf_op jit(solution)/shard_map/ppermute | solution.py:34
  58.5 18.5 %all-reduce.2 = (f32[16]{0:T(128)S(1)}, f32[16]{0:T(128)S(1)}) all-reduce(f32[16]{0:T(128)S(1)} %dynamic-update-slice, f32[16]{0:T(128)S(1)} %dynamic-update-slice.1), channel_id=3, replica_groups=mesh['sp'=8,'tp'=4] {'sp'}, use_global_device_ids=true, to_apply=%add | all-reduce | flops 32 | bytes 256
  78.3 17.4 %all-gather.5 = f32[8,32,2]{1,2,0:T(2,128)S(1)} all-gather(f32[1,32,2]{1,2,0:T(2,128)S(1)} %bitcast.321), channel_id=1, replica_groups=mesh['sp'=8,'tp'=4] {'sp'}, dimensions={0}, use_global_device_ids=true | all-gather | bytes 2304 | tf_op jit(solution)/shard_map/all_gather | solution.py:174
  96.5 4.2 %copy.69 = f32[2,2,512,256]{2,1,3,0:T(2,128)} copy(f32[2,2,512,256]{3,2,0,1:T(8,128)} %bitcast.301) | data formatting | bytes 4194304 | tf_op jit(solution)/shard_map/transpose | solution.py:158
  100.7 4.0 %reshape.448 = f32[2,1024,256]{1,2,0:T(8,128)} reshape(f32[2,2,512,256]{2,1,3,0:T(2,128)} %copy.69) | data formatting | bytes 4194304 | tf_op jit(solution)/shard_map/reshape | solution.py:158
  107.5 26.3 %all-gather.4 = f32[8,2,256]{2,1,0:T(2,128)S(1)} all-gather(f32[1,2,256]{2,1,0:T(2,128)S(1)} %bitcast.316), channel_id=5, replica_groups=mesh['sp'=8,'tp'=4] {'sp'}, dimensions={0}, use_global_device_ids=true | all-gather | bytes 18432 | tf_op jit(solution)/shard_map/all_gather | solution.py:19
  135.2 31.1 %all_gather.38 = f32[2,256,256]{2,1,0:T(8,128)} all-gather(f32[2,32,256]{2,1,0:T(8,128)S(1)} %copy-done.12), channel_id=1, replica_groups=mesh['sp'=8,'tp'=4] {'sp'}, dimensions={1}, use_global_device_ids=true | all-gather | bytes 589824 | tf_op jit(solution)/shard_map/all_gather | solution.py:173
  166.3 2.1 iota_compare_fusion.1
  169.3 5.5 %fusion.117 = f32[2,128,1024]{2,1,0:T(8,128)} fusion(bf16[1024,2,128]{0,2,1:T(8,128)(2,1)S(1)} %bitcast.309, bf16[1280,2,128]{0,2,1:T(8,128)(2,1)} %bitcast.310, s32[2,1024]{1,0:T(2,128)S(1)} %iota_subtract_fusion, s32[1280]{0:T(1024)S(1)} %iota_add_fusion, pred[1024,1280]{1,0:T(8,128)(4,1)} %iota_compare_fusion.1, f32[1024,2]{0,1:T(2,128)S(1)} %copy-done.17, ...), kind=kOutput, calls=%fused_computation.142 | convolution fusion | flops 744488960 | bytes 3625988 | tf_op jit(solution)/shard_map/tgc,gce->tge/dot_general | solution.py:230
  174.9 2.5 copy.77
  177.4 9.4 %while.42 = (s32[]{:T(128)}, f32[2,256,256]{2,1,0:T(8,128)S(1)}, f32[2,256]{1,0:T(2,128)S(1)}, f32[2]{0:T(128)S(1)}, f32[2]{0:T(128)S(1)}, /*index=5*/s32[]{:T(1...) while((s32[]{:T(128)}, f32[2,256,256]{2,1,0:T(8,128)S(1)}, ...), condition=%wide.region_13.14_spmd.clone, body=%wide.region_12.13_spmd.clone.sunk | while | flops 657944 | bytes 1579293 | solution.py:28
  186.9 2.1 fusion.109
  189.2 4.8 %multiply_reduce_fusion = (f32[1024]{0:T(1024)S(1)}, f32[2,1024,256]{1,2,0:T(8,128)}) fusion(f32[2,1024]{1,0:T(2,128)S(1)} %get-tuple-element.383, f32[2,256,256]{2,1,0:T(8,128)S(1)} %copy-done.11, f32[2,256,256]{2,1,0:T(8,128)S(1)} %get-tuple-element.251, f32[2]{0:T(128)S(1)} %subtract_exponential_fusion.5, f32[2]{0:T(128)S(1)} %get-tuple-element.385, ...), kind=kOutput, calls=%fused_computation.118 | convolution fusion | flops 1614150656 | bytes 6320144 | tf_op jit(solution)/shard_map/hld,hde->hle/dot_general | solution.py:190
  194.0 5.6 %psum.7 = f32[1024]{0:T(1024)S(1)} all-reduce(f32[1024]{0:T(1024)S(1)} %get-tuple-element.398), channel_id=1, replica_groups=mesh['sp'=8,'tp'=4] {'tp'}, use_global_device_ids=true, to_apply=%region_15.16 | all-reduce | flops 1024 | bytes 8192 | tf_op jit(solution)/shard_map/psum | solution.py:198
  199.6 11.7 %fusion.103 = f32[1024,2048,1]{1,0,2:T(8,128)} fusion(bf16[2,256,2048]{2,1,0:T(8,128)(2,1)S(1)} %bitcast.298, f32[2,1024,256]{1,2,0:T(8,128)} %get-tuple-element.399, bf16[256,2,8,256]{3,2,1,0:T(8,128)(2,1)} %bitcast.325, bf16[1024,2048]{1,0:T(8,128)(2,1)} %copy-done.1, f32[2,256]{1,0:T(2,128)S(1)} %copy-done.19, f32[1024]{0:T(1024)S(1)} %add_rsqrt_fusion), kind=kOutput, calls=%fused_computation.126 | convolution fusion | flops 4299161600 | bytes 18880512 | tf_op jit(solution)/shard_map/hte,hed->td/dot_general | solution.py:239
  211.4 11.6 %fusion.51 = bf16[1024,2048]{1,0:T(8,128)(2,1)} fusion(f32[1024,2048,1]{1,0,2:T(8,128)} %fusion.103, bf16[256,2048]{1,0:T(8,128)(2,1)} %param.44, f32[1024,256]{1,0:T(8,128)S(1)} %copy-done.7, f32[256]{0:T(256)S(1)} %copy-done.18, bf16[1024,2048]{1,0:T(8,128)(2,1)} %copy-done.1, bf16[2048,256]{1,0:T(8,128)(2,1)} %param.40), kind=kOutput, calls=%fused_computation.86 | convolution fusion | flops 2153512960 | bytes 19923968 | tf_op jit(solution)/shard_map/dot_general | solution.py:243
  223.0 48.8 %reduce-scatter.2.cloned.1.call-done = bf16[256,2048]{1,0:T(8,128)(2,1)} async-done(((bf16[1024,2048]{1,0:T(8,128)(2,1)}), bf16[256,2048]{1,0:T(8,128)(2,1)}) %reduce-scatter.2.cloned.1.call-update) | async-done | bytes 1048592 | tf_op jit(solution)/shard_map/reduce_scatter | solution.py:242
  271.8 1.5 fusion.63
  273.3 2.5 fusion.65
  (185 shorter events, 36.8 us)
Async XLA Ops:
  6.5 193.1 %copy-start = (bf16[512,2048]{1,0:T(8,128)(2,1)S(1)}, bf16[512,2048]{1,0:T(8,128)(2,1)}, u32[]{:S(2)}) copy-start(bf16[512,2048]{1,0:T(8,128)(2,1)} %param.43) | copy-start | bytes 6291460
  6.5 170.9 %all-gather.8.cloned.1.call-start = ((), (), s32[]{:S(2)}) async-start(), calls=%async_computation.2 | async-start | bytes 4718592 | tf_op jit(solution)/shard_map/all_gather | solution.py:19
  8.2 3.4 %copy-start.6 = (bf16[1024,2048]{1,0:T(8,128)(2,1)S(1)}, bf16[1024,2048]{1,0:T(8,128)(2,1)}, u32[]{:S(2)}) copy-start(bf16[1024,2048]{1,0:T(8,128)(2,1)} %param.25) | copy-start | bytes 12582916
  8.2 3.4 %copy-start.14 = (f32[2048]{0:T(1024)S(1)}, f32[2048]{0:T(1024)}, u32[]{:S(2)}) copy-start(f32[2048]{0:T(1024)} %param.26) | copy-start | bytes 24580
  11.6 1.6 copy-start.21
  12.7 12.3 %copy-start.1 = (bf16[1024,2048]{1,0:T(8,128)(2,1)}, bf16[1024,2048]{1,0:T(8,128)(2,1)S(1)}, u32[]{:S(2)}) copy-start(bf16[1024,2048]{1,0:T(8,128)(2,1)S(1)} %fusion.50) | copy-start | bytes 12582916
  13.2 2.5 copy-start.22
  15.5 7.9 %copy-start.8 = (bf16[1024,2,256]{2,0,1:T(8,128)(2,1)}, bf16[1024,2,256]{2,0,1:T(8,128)(2,1)S(1)}, u32[]{:S(2)}) copy-start(bf16[1024,2,256]{2,0,1:T(8,128)(2,1)S(1)} %fusion.89) | copy-start | bytes 3145732
  15.7 2.3 copy-start.23
  23.4 1.5 copy-start.13
  32.4 2.4 copy-start.5
  32.4 3.0 %copy-start.9 = (f32[2,2,512,256]{3,2,1,0:T(8,128)S(1)}, f32[2,2,512,256]{3,2,1,0:T(8,128)}, u32[]{:S(2)}) copy-start(f32[2,2,512,256]{3,2,1,0:T(8,128)} %get-tuple-element.595) | copy-start | bytes 6291460 | tf_op jit(solution)/shard_map/while
  34.7 1.2 copy-start.4
  35.3 1.3 copy-start.3
  36.6 1.3 copy-start.10
  43.1 2.4 copy-start.5
  43.1 3.0 %copy-start.9 = (f32[2,2,512,256]{3,2,1,0:T(8,128)S(1)}, f32[2,2,512,256]{3,2,1,0:T(8,128)}, u32[]{:S(2)}) copy-start(f32[2,2,512,256]{3,2,1,0:T(8,128)} %get-tuple-element.595) | copy-start | bytes 6291460 | tf_op jit(solution)/shard_map/while
  45.4 1.2 copy-start.4
  46.1 1.3 copy-start.3
  47.4 1.3 copy-start.10
  49.5 222.3 %reduce-scatter.2.cloned.1.call-start = ((), (), s32[]{:S(2)}) async-start(), calls=%async_computation.1 | async-start | bytes 5242880 | tf_op jit(solution)/shard_map/reduce_scatter | solution.py:242
  49.6 3.8 %copy-start.24 = (u32[32]{0:T(128)S(1)}, u32[32]{0:T(128)}, u32[]{:S(2)}) copy-start(u32[32]{0:T(128)} %constant.118) | copy-start | bytes 388
  49.6 28.8 %copy-start.20 = (f32[2,32]{1,0:T(2,128)S(1)}, f32[2,32]{1,0:T(2,128)}, u32[]{:S(2)}) copy-start(f32[2,32]{1,0:T(2,128)} %param.37) | copy-start | bytes 772
  55.0 113.4 %collective-permute-start = (bf16[256,256]{0,1:T(8,128)(2,1)S(1)}, bf16[256,256]{0,1:T(8,128)(2,1)S(1)}, u32[]{:S(2)}, u32[]{:S(2)}) collective-permute-start(bf16[256,256]{0,1:T(8,128)(2,1)S(1)} %slice.27), channel_id=1, source_target_pairs={{0,4},{4,8},{8,12},{12,16},{16,20},{20,24},{24,28},{1,5},{5,9},{9,... | collective-permute-start | bytes 393224 | tf_op jit(solution)/shard_map/ppermute | solution.py:34
  100.7 34.5 %copy-start.12 = (f32[2,32,256]{2,1,0:T(8,128)S(1)}, f32[2,32,256]{2,1,0:T(8,128)}, u32[]{:S(2)}) copy-start(f32[2,32,256]{2,1,0:T(8,128)} %param.36) | copy-start | bytes 196612
  135.2 34.1 %copy-start.17 = (f32[1024,2]{0,1:T(2,128)S(1)}, f32[1024,2]{0,1:T(2,128)}, u32[]{:S(2)}) copy-start(f32[1024,2]{0,1:T(2,128)} %minimum_convert_fusion) | copy-start | bytes 24580
  177.4 9.4 %copy-start.16 = (f32[256,2]{0,1:T(2,128)S(1)}, f32[256,2]{0,1:T(2,128)}, u32[]{:S(2)}) copy-start(f32[256,2]{0,1:T(2,128)} %reshape.474) | copy-start | bytes 6148
  177.4 11.8 %copy-start.11 = (f32[2,256,256]{2,1,0:T(8,128)S(1)}, f32[2,256,256]{2,1,0:T(8,128)}, u32[]{:S(2)}) copy-start(f32[2,256,256]{2,1,0:T(8,128)} %all_gather.38) | copy-start | bytes 1572868
  189.2 10.4 %copy-start.19 = (f32[2,256]{1,0:T(2,128)S(1)}, f32[2,256]{1,0:T(2,128)}, u32[]{:S(2)}) copy-start(f32[2,256]{1,0:T(2,128)} %mul.312) | copy-start | bytes 6148
  199.6 11.7 %copy-start.7 = (f32[1024,256]{1,0:T(8,128)S(1)}, f32[1024,256]{1,0:T(8,128)}, u32[]{:S(2)}) copy-start(f32[1024,256]{1,0:T(8,128)} %copy.77) | copy-start | bytes 3145732
  199.6 11.7 %copy-start.18 = (f32[256]{0:T(256)S(1)}, f32[256]{0:T(256)}, u32[]{:S(2)}) copy-start(f32[256]{0:T(256)} %dynamic_slice.72) | copy-start | bytes 3076
  223.0 50.4 %copy-start.15 = (f32[2048]{0:T(1024)S(1)}, f32[2048]{0:T(1024)}, u32[]{:S(2)}) copy-start(f32[2048]{0:T(1024)} %param.45) | copy-start | bytes 24580
  (1 other events, 0.8 us)
Sparse Core Ops, SparseCore 0:
  49.6 74.8 all-gather.7
  223.1 48.6 reduce-scatter.1
where the time goes:
time: 286 us; the launch traced here: 283 us
  blocking collectives  98.9 us (35%)
  matrix products  62.1 us (22%)
  waiting for transfers between devices  48.8 us (17%)
  other arithmetic  29.9 us (10%)
  local copies, waits for them, and re-layouts  24.6 us (9%)
  between operations  14.3 us (5%)
  starting transfers between devices  3.49 us (1%)
    reduce_scatter x1, waiting for transfers between devices, body(): lax.psum_scatter((memory_term + jnp.dot(pool_out, w_out_pool, preferred_e...  48.8 us
    all_gather x1, blocking collectives, body(): lax.all_gather(initial_memory, 'sp', axis=1, tiled=True)  31.1 us
    all_gather x1, blocking collectives, prefix_2(): pieces = jax.tree.map(lambda part: lax.all_gather(part, axis), value)  26.3 us
    unnamed x1, blocking collectives  18.5 us
    all_gather x1, blocking collectives, body(): lax.all_gather(initial_normal, 'sp', axis=1, tiled=True)  17.4 us
    dot_general x1, matrix products, body(): jnp.einsum('hte,hed->td', memory_out, out_memory, preferred_element_type=...  11.7 us
    dot_general x1, matrix products, body(): jnp.dot(pool_out, w_out_pool, preferred_element_type=jnp.float32)  11.6 us
    select_n x21, other arithmetic, lap(): jnp.where(position < mine, new, old)  9.07 us
  transfers between devices with their start and end apart: 3, of which 1 were waited for; matrix products, arithmetic and copies ran while one was open for 11% of the time, Pallas kernels for 0%

commit v1 on v0

v1 whole, which is shorter than its diff:
```python
import functools

import jax
import jax.numpy as jnp
from jax import lax
from jax.experimental import pallas as pl
from jax.experimental.pallas import tpu as pltpu
from jax.sharding import PartitionSpec as P

HEAD_DIM = 256
GROUP_DIM = 128
WIDEST = 256
TILE = 256
CHUNKS = 2
EPS = 1e-06
FLOOR = -1e30
F32 = jnp.float32
BF16 = jnp.bfloat16
MESH = pl.DeviceIdType.MESH


def dot(a, b):
    return jnp.dot(a, b, preferred_element_type=F32)


def silu(x):
    return x / (1.0 + jnp.exp(-x))


def kernel(
    n_sp,
    n_tp,
    tokens_hbm,
    gain_ref,
    wq_hbm,
    wk_hbm,
    wv_hbm,
    wg_hbm,
    gates_w_ref,
    gates_b_ref,
    extra_ref,
    init_ref,
    normal_ref,
    mem_gain_ref,
    wpi_hbm,
    wpg_hbm,
    mix_ref,
    pool_gain_ref,
    wom_hbm,
    wop_hbm,
    post_ref,
    out_ref,
    tokens,
    wq,
    wk,
    wv,
    wg,
    wpi,
    wpg,
    wom,
    wop,
    normed,
    q_ref,
    k_ref,
    v_ref,
    gate_ref,
    pgate_ref,
    ext_ref,
    pool_ref,
    rows_ref,
    cols_ref,
    num_ref,
    den_ref,
    max_ref,
    s_send,
    s_recv,
    a_send,
    a_recv,
    e_send,
    e_recv,
    sq_send,
    sq_recv,
    scale_ref,
    sib_send,
    sib_recv,
    own_ref,
    link_send,
    link_recv,
    local_sem,
    s_sems,
    a_sems,
    e_sems,
    halo_sems,
    sq_sems,
    sib_sems,
    link_sems,
):
    T, D = tokens.shape
    H = q_ref.shape[0]
    G = pool_ref.shape[1] // GROUP_DIM
    sp = lax.axis_index("sp")
    tp = lax.axis_index("tp")
    head_scale = HEAD_DIM ** (-0.5)
    tiles = T // TILE

    loads = {}
    for slot, (name, src, dst) in enumerate(
        [
            ("tokens", tokens_hbm, tokens),
            ("wk", wk_hbm, wk),
            ("wv", wv_hbm, wv),
            ("wpi", wpi_hbm, wpi),
            ("wq", wq_hbm, wq),
            ("wg", wg_hbm, wg),
            ("wpg", wpg_hbm, wpg),
            ("wop", wop_hbm, wop),
            ("wom", wom_hbm, wom),
        ]
    ):
        loads[name] = pltpu.make_async_copy(src, dst, local_sem.at[slot])
        loads[name].start()

    barrier = pltpu.get_barrier_semaphore()
    for step in range(1, n_sp):
        pl.semaphore_signal(
            barrier, inc=1, device_id={"sp": lax.rem(sp + step, n_sp)}, device_id_type=MESH
        )
    for step in range(1, n_tp):
        pl.semaphore_signal(
            barrier, inc=1, device_id={"tp": lax.rem(tp + step, n_tp)}, device_id_type=MESH
        )

    def remote(src, dst, sems, slot, axis, peer):
        return pltpu.make_async_remote_copy(
            src_ref=src,
            dst_ref=dst,
            send_sem=sems.at[0, slot],
            recv_sem=sems.at[1, slot],
            device_id={axis: peer},
            device_id_type=MESH,
        )

    def by_tile(body, size=TILE):
        def step(index, carry):
            body(pl.ds(pl.multiple_of(index * size, size), size))
            return carry

        lax.fori_loop(0, T // size, step, 0)

    loads["tokens"].wait()

    def norm_tile(rows):
        x = tokens[rows, :].astype(F32)
        scale = lax.rsqrt(jnp.mean(x * x, axis=-1, keepdims=True) + EPS)
        normed[rows, :] = (x * scale * gain_ref[...]).astype(BF16)

    by_tile(norm_tile, 64)

    def gate_tile(rows):
        cols_ref[rows, :] = dot(normed[rows, :], gates_w_ref[...]) + gates_b_ref[...]

    by_tile(gate_tile)
    tri = (
        lax.broadcasted_iota(jnp.int32, (TILE, TILE), 0)
        <= lax.broadcasted_iota(jnp.int32, (TILE, TILE), 1)
    ).astype(F32)
    rows_ref[...] = jnp.zeros_like(rows_ref)
    carry = jnp.zeros((8, 1), F32)
    for t in range(tiles):
        span = pl.ds(t * TILE, TILE)
        raw = cols_ref[span, :].T[0:8]
        log_keep = jnp.minimum(raw, 0.0) - jnp.log1p(jnp.exp(-jnp.abs(raw))) + extra_ref[:, span]
        run = carry + jnp.dot(
            log_keep, tri, preferred_element_type=F32, precision=lax.Precision.HIGHEST
        )
        carry = run[:, TILE - 1 : TILE]
        rows_ref[0:H, span] = raw[0:H] - run[H : 2 * H]
        rows_ref[H : 2 * H, span] = run[H : 2 * H]
    for t in range(tiles):
        span = pl.ds(t * TILE, TILE)
        cols_ref[span, :] = rows_ref[:, span].T

    def project(name, weight, store):
        loads[name].wait()

        def tile(rows):
            store(rows, dot(normed[rows, :], weight[...]))

        by_tile(tile)

    def heads_to(ref):
        def store(rows, value):
            for h in range(H):
                ref[h, rows, :] = value[:, h * HEAD_DIM : (h + 1) * HEAD_DIM].astype(ref.dtype)

        return store

    project("wk", wk, heads_to(k_ref))
    project("wv", wv, heads_to(v_ref))

    part = HEAD_DIM // n_sp
    a_send[...] = jnp.zeros_like(a_send)
    for h in range(H):
        a_max = jnp.max(rows_ref[h : h + 1, :], axis=-1, keepdims=True)
        total = rows_ref[H + h : H + h + 1, T - 1 : T]
        state = jnp.zeros((HEAD_DIM, HEAD_DIM), F32)
        normal = jnp.zeros((1, HEAD_DIM), F32)
        for t in range(tiles):
            span = pl.ds(t * TILE, TILE)
            weight = jnp.exp(cols_ref[span, h : h + 1] - a_max)
            kw = weight * k_ref[h, span, :].astype(F32)
            normal = normal + jnp.sum(kw, axis=0, keepdims=True)
            state = state + lax.dot_general(
                kw.astype(BF16),
                v_ref[h, span, :],
                (((0,), (0,)), ((), ())),
                preferred_element_type=F32,
            )
        s_send[:, h] = state.reshape(n_sp, part, HEAD_DIM).astype(s_send.dtype)
        a_send[4 * h : 4 * h + 1, :] = jnp.broadcast_to(total + a_max, (1, HEAD_DIM))
        a_send[4 * h + 1 : 4 * h + 2, :] = jnp.broadcast_to(total, (1, HEAD_DIM))
        a_send[4 * h + 2 : 4 * h + 3, :] = normal
        a_send[4 * h + 3 : 4 * h + 4, :] = normal_ref[h : h + 1, :]

    pl.semaphore_wait(barrier, n_sp - 1 + n_tp - 1)
    first = []
    for step in range(1, n_sp):
        peer = lax.rem(sp + step, n_sp)
        first.append(remote(s_send.at[peer], s_recv.at[sp], s_sems, step, "sp", peer))
        first.append(remote(a_send, a_recv.at[sp], a_sems, step, "sp", peer))
    for copy in first:
        copy.start()
    s_recv[sp] = s_send[sp]
    a_recv[sp] = a_send[...]

    def store_pool(rows, value):
        ext_ref[pl.ds(pl.multiple_of(rows.start + WIDEST, TILE), TILE), :] = value.astype(BF16)

    project("wpi", wpi, store_pool)
    halo = remote(
        ext_ref.at[pl.ds(T, WIDEST)],
        ext_ref.at[pl.ds(0, WIDEST)],
        halo_sems,
        0,
        "sp",
        lax.rem(sp + 1, n_sp),
    )
    halo.start()
    project("wq", wq, heads_to(q_ref))
    project("wg", wg, heads_to(gate_ref))

    for copy in first:
        copy.wait()
    enter_max, enter_normal = [], []
    for h in range(H):
        state = init_ref[h].astype(F32)
        normal = jnp.zeros((1, HEAD_DIM), F32)
        for j in range(n_sp):
            normal = normal + a_recv[j, 4 * h + 3 : 4 * h + 4, :]
        stab = jnp.zeros((1, HEAD_DIM), F32)
        my_stab, my_normal = stab, normal
        for j in range(n_sp):
            e_send[j, h] = state.astype(e_send.dtype)
            my_stab = jnp.where(sp == j, stab, my_stab)
            my_normal = jnp.where(sp == j, normal, my_normal)
            late = a_recv[j, 4 * h : 4 * h + 1, :]
            keep = a_recv[j, 4 * h + 1 : 4 * h + 2, :]
            joint = jnp.maximum(late, keep + stab)
            early_factor = jnp.exp(keep + stab - joint)
            late_factor = jnp.exp(late - joint)
            state = state * early_factor + s_recv[j, h].astype(F32) * late_factor
            normal = normal * early_factor + a_recv[j, 4 * h + 2 : 4 * h + 3, :] * late_factor
            stab = joint
        enter_max.append(my_stab[:, 0:1])
        enter_normal.append(my_normal)
    second = []
    for step in range(1, n_sp):
        peer = lax.rem(sp + step, n_sp)
        second.append(remote(e_send.at[peer], e_recv.at[sp], e_sems, step, "sp", peer))
    for copy in second:
        copy.start()
    e_recv[sp] = e_send[sp]

    for h in range(H):
        for t in range(tiles):
            span = pl.ds(t * TILE, TILE)
            width = (t + 1) * TILE
            decayed = cols_ref[span, H + h : H + h + 1] + rows_ref[h : h + 1, 0:width]
            causal = (
                lax.broadcasted_iota(jnp.int32, (TILE, width), 0) + t * TILE
                >= lax.broadcasted_iota(jnp.int32, (TILE, width), 1)
            )
            decayed = jnp.where(causal, decayed, FLOOR)
            row_max = jnp.max(decayed, axis=-1, keepdims=True)
            scores = lax.dot_general(
                q_ref[h, span, :],
                k_ref[h, 0:width, :],
                (((1,), (1,)), ((), ())),
                preferred_element_type=F32,
            )
            weights = jnp.exp(decayed - row_max) * scores * head_scale
            den_ref[h, span, :] = jnp.sum(weights, axis=-1, keepdims=True)
            max_ref[h, span, :] = row_max
            num_ref[h, span, :] = dot(weights.astype(BF16), v_ref[h, 0:width, :])

    def store_gate(rows, value):
        pgate_ref[rows, :] = value

    project("wpg", wpg, store_gate)
    halo.wait()
    for g in range(G):
        window = jnp.left_shift(2, tp * G + g)
        offset = (
            lax.broadcasted_iota(jnp.int32, (TILE, TILE + WIDEST), 0)
            + WIDEST
            - lax.broadcasted_iota(jnp.int32, (TILE, TILE + WIDEST), 1)
        )
        band = jnp.where((offset >= 0) & (offset < window), 1.0, 0.0).astype(BF16)
        lanes = slice(g * GROUP_DIM, (g + 1) * GROUP_DIM)
        for t in range(tiles):
            span = pl.ds(t * TILE, TILE)
            here = ext_ref[t * TILE + WIDEST : (t + 1) * TILE + WIDEST, lanes]
            before = ext_ref[t * TILE : t * TILE + WIDEST, lanes]
            if t == 0:
                before = jnp.where(sp > 0, before.astype(F32), 0.0).astype(BF16)
            sums = dot(band[:, :WIDEST], before) + dot(band[:, WIDEST:], here)
            position = lax.broadcasted_iota(jnp.int32, (TILE, 1), 0) + (sp * T + t * TILE + 1)
            counts = jnp.minimum(position, window).astype(F32)
            pooled = (sums / counts - here.astype(F32)).astype(BF16)
            mixed = dot(pooled, mix_ref[g])
            pool_ref[span, lanes] = (
                mixed * pool_gain_ref[:, lanes] * silu(pgate_ref[span, lanes])
            ).astype(BF16)

    for copy in second:
        copy.wait()
    for t in range(tiles):
        span = pl.ds(t * TILE, TILE)
        squares = jnp.zeros((TILE, 1), F32)
        for h in range(H):
            state = e_recv[:, h].reshape(HEAD_DIM, HEAD_DIM).astype(BF16)
            queries = q_ref[h, span, :]
            carried = cols_ref[span, H + h : H + h + 1] + enter_max[h]
            row_max = max_ref[h, span, :]
            joint = jnp.maximum(row_max, carried)
            local_weight = jnp.exp(row_max - joint)
            carry_weight = jnp.exp(carried - joint) * head_scale
            numerator = num_ref[h, span, :] * local_weight + carry_weight * dot(queries, state)
            denominator = den_ref[h, span, :] * local_weight + carry_weight * jnp.sum(
                queries.astype(F32) * enter_normal[h], axis=-1, keepdims=True
            )
            memory = numerator / jnp.maximum(jnp.abs(denominator), jnp.exp(-joint))
            num_ref[h, span, :] = memory
            squares = squares + jnp.sum(memory * memory, axis=-1, keepdims=True)
        sq_send[:, span] = jnp.broadcast_to(squares, (TILE, 128)).T[0:8]

    third = []
    for step in range(1, n_tp):
        peer = lax.rem(tp + step, n_tp)
        third.append(remote(sq_send, sq_recv.at[step], sq_sems, step, "tp", peer))
    for copy in third:
        copy.start()
    loads["wop"].wait()
    loads["wom"].wait()
    for copy in third:
        copy.wait()
    for t in range(tiles):
        span = pl.ds(t * TILE, TILE)
        total = sq_send[0:1, span]
        for step in range(1, n_tp):
            total = total + sq_recv[step, 0:1, span]
        scale = lax.rsqrt(total / (HEAD_DIM * H * n_tp) + EPS)
        scale_ref[span, :] = jnp.broadcast_to(scale, (128, TILE)).T

    chips = n_tp // 2
    chip, core = tp // 2, lax.rem(tp, 2)
    sibling = chip * 2 + 1 - core
    block = T // n_tp
    size = block // CHUNKS

    def memory_out(rows):
        parts = []
        for h in range(H):
            lanes = slice(h * HEAD_DIM, (h + 1) * HEAD_DIM)
            parts.append(
                (
                    num_ref[h, rows, :]
                    * scale_ref[rows, 0:1]
                    * mem_gain_ref[:, lanes]
                    * silu(gate_ref[h, rows, :])
                ).astype(BF16)
            )
        return parts[0] if H == 1 else jnp.concatenate(parts, axis=1)

    links, siblings = [], []
    for j in range(1, chips + 1):
        target = lax.rem(chip + j, chips)
        for n in range(CHUNKS):
            slot = (j - 1) * CHUNKS + n
            theirs = pl.ds(
                pl.multiple_of((target * 2 + 1 - core) * block + n * size, size), size
            )
            ours = pl.ds(pl.multiple_of((target * 2 + core) * block + n * size, size), size)
            lhs_memory = jnp.concatenate([memory_out(theirs), memory_out(ours)], axis=0)
            lhs_pool = jnp.concatenate([pool_ref[theirs, :], pool_ref[ours, :]], axis=0)
            both = (dot(lhs_memory, wom[...]) + dot(lhs_pool, wop[...])).astype(BF16)
            sib_send[slot] = both[:size]
            own_ref[slot] = both[size:]
            copy = remote(
                sib_send.at[slot], sib_recv.at[slot], sib_sems, slot, "tp", sibling
            )
            copy.start()
            siblings.append(copy)
            if j < chips:
                copy.wait_recv()
                link_send[slot] = (
                    own_ref[slot].astype(F32) + sib_recv[slot].astype(F32)
                ).astype(BF16)
                hop = remote(
                    link_send.at[slot],
                    link_recv.at[slot],
                    link_sems,
                    slot,
                    "tp",
                    target * 2 + core,
                )
                hop.start()
                links.append(hop)
    for n in range(CHUNKS):
        slot = (chips - 1) * CHUNKS + n
        siblings[slot].wait_recv()
        total = own_ref[slot].astype(F32) + sib_recv[slot].astype(F32)
        for j in range(1, chips):
            other = (j - 1) * CHUNKS + n
            links[other].wait_recv()
            total = total + link_recv[other].astype(F32)
        scale = lax.rsqrt(jnp.mean(total * total, axis=-1, keepdims=True) + EPS)
        out_ref[pl.ds(n * size, size), :] = (total * scale * post_ref[...]).astype(BF16)
    for copy in siblings + links:
        copy.wait_send()


def body(
    n_sp,
    n_tp,
    tokens,
    pre_gain,
    w_query,
    w_key,
    w_value,
    memory_output_gate_weight,
    w_input_gate,
    w_forget_gate,
    input_bias,
    forget_bias,
    forget_extra,
    initial_memory,
    initial_normal,
    memory_gain,
    w_pool_input,
    w_pool_gate,
    pool_mix,
    pool_gain,
    w_out_memory,
    w_out_pool,
    post_gain,
):
    T, D = tokens.shape
    MW = w_query.shape[1]
    PW = w_pool_input.shape[1]
    H = MW // HEAD_DIM
    G = PW // GROUP_DIM
    sp, tp = lax.axis_index("sp"), lax.axis_index("tp")
    cut = functools.partial(lax.dynamic_slice_in_dim, start_index=tp * H, slice_size=H)
    gates_w = jnp.pad(
        jnp.concatenate([cut(w_input_gate, axis=1), cut(w_forget_gate, axis=1)], axis=1),
        ((0, 0), (0, 128 - 2 * H)),
    )
    gates_b = jnp.pad(
        jnp.concatenate([cut(input_bias, axis=0), cut(forget_bias, axis=0)]), (0, 128 - 2 * H)
    )[None]
    extra = jnp.pad(forget_extra.T, ((H, 8 - 2 * H), (0, 0)))
    part = initial_normal.shape[1]
    normal = lax.dynamic_update_slice(
        jnp.zeros((H, HEAD_DIM), F32), initial_normal, (0, sp * part)
    )
    mem_gain = lax.dynamic_slice_in_dim(memory_gain, tp * MW, MW, 0)[None]
    gain_pool = lax.dynamic_slice_in_dim(pool_gain, tp * PW, PW, 0)[None]
    mix = lax.dynamic_slice_in_dim(pool_mix, tp * G, G, 0)
    wire = BF16 if part % 16 == 0 else F32
    chips = n_tp // 2
    block = T // n_tp
    slots = chips * CHUNKS
    size = block // CHUNKS
    hbm = pl.BlockSpec(memory_space=pl.ANY)
    vmem = pl.BlockSpec(memory_space=pltpu.VMEM)
    V = pltpu.VMEM
    dma = pltpu.SemaphoreType.DMA
    return pl.pallas_call(
        functools.partial(kernel, n_sp, n_tp),
        out_shape=jax.ShapeDtypeStruct((block, D), BF16),
        in_specs=[hbm, vmem, hbm, hbm, hbm, hbm, vmem, vmem, vmem, vmem, vmem, vmem]
        + [hbm, hbm, vmem, vmem, hbm, hbm, vmem],
        out_specs=vmem,
        scratch_shapes=[
            V((T, D), BF16),
            V((D, MW), BF16),
            V((D, MW), BF16),
            V((D, MW), BF16),
            V((D, MW), BF16),
            V((D, PW), BF16),
            V((D, PW), BF16),
            V((MW, D), BF16),
            V((PW, D), BF16),
            V((T, D), BF16),
            V((H, T, HEAD_DIM), BF16),
            V((H, T, HEAD_DIM), BF16),
            V((H, T, HEAD_DIM), BF16),
            V((H, T, HEAD_DIM), F32),
            V((T, PW), F32),
            V((T + WIDEST, PW), BF16),
            V((T, PW), BF16),
            V((128, T), F32),
            V((T, 128), F32),
            V((H, T, HEAD_DIM), F32),
            V((H, T, 1), F32),
            V((H, T, 1), F32),
            V((n_sp, H, part, HEAD_DIM), wire),
            V((n_sp, H, part, HEAD_DIM), wire),
            V((8, HEAD_DIM), F32),
            V((n_sp, 8, HEAD_DIM), F32),
            V((n_sp, H, part, HEAD_DIM), wire),
            V((n_sp, H, part, HEAD_DIM), wire),
            V((8, T), F32),
            V((n_tp, 8, T), F32),
            V((T, 128), F32),
            V((slots, size, D), BF16),
            V((slots, size, D), BF16),
            V((slots, size, D), BF16),
            V((slots, size, D), BF16),
            V((slots, size, D), BF16),
            dma((9,)),
            dma((2, n_sp)),
            dma((2, n_sp)),
            dma((2, n_sp)),
            dma((2, 1)),
            dma((2, n_tp)),
            dma((2, slots)),
            dma((2, slots)),
        ],
        compiler_params=pltpu.CompilerParams(
            collective_id=0, has_side_effects=True, vmem_limit_bytes=60 * 1024 * 1024
        ),
    )(
        tokens,
        pre_gain[None],
        w_query,
        w_key,
        w_value,
        memory_output_gate_weight,
        gates_w,
        gates_b,
        extra,
        initial_memory,
        normal,
        mem_gain,
        w_pool_input,
        w_pool_gate,
        mix,
        gain_pool,
        w_out_memory,
        w_out_pool,
        post_gain[None],
    )


def solution(mesh):
    in_specs = (
        P("sp", None),
        P(),
        P(None, "tp"),
        P(None, "tp"),
        P(None, "tp"),
        P(None, "tp"),
        P(),
        P(),
        P(),
        P(),
        P("sp", "tp"),
        P("tp", "sp", None),
        P("tp", "sp"),
        P(),
        P(None, "tp"),
        P(None, "tp"),
        P(),
        P(),
        P("tp", None),
        P("tp", None),
        P(),
    )
    out_specs = P(("sp", "tp"), None)
    sizes = dict(mesh.shape)
    run = functools.partial(body, sizes["sp"], sizes["tp"])
    return jax.shard_map(run, mesh=mesh, in_specs=in_specs, out_specs=out_specs, check_vma=False)
```

time: 286 us -> 86.2 us (0.30); the launches traced: 283 us -> 85.8 us
  blocking collectives: 98.9 us -> 0 us
  Pallas kernels: 0 us -> 73.9 us
  matrix products: 62.1 us -> 0 us
  waiting for transfers between devices: 48.8 us -> 0 us
  other arithmetic: 29.9 us -> 0.6 us
  between operations: 14.3 us -> 0.03 us
  local copies, waits for them, and re-layouts: 24.6 us -> 11.3 us
  starting transfers between devices: 3.49 us -> 0 us
    all_gather x3 -> x0, blocking collectives: 74.8 us -> none  [the longest x1 31.1 us: body(): lax.all_gather(initial_memory, 'sp', axis=1, tiled=True)]
    pallas_call x0 -> x1, Pallas kernels: none -> 73.9 us  [body(): pl.pallas_call(functools.partial(kernel, n_sp, n_tp), out_shape=jax.Shape...]
    dot_general x21 -> x0, matrix products: 62.1 us -> none  [the longest x1 11.7 us: body(): jnp.einsum('hte,hed->td', memory_out, out_memory, preferred_element_type=...]
    reduce_scatter x1 -> x0, waiting for transfers between devices: 48.8 us -> none  [body(): lax.psum_scatter((memory_term + jnp.dot(pool_out, w_out_pool, preferred_e...]
    unnamed x1 -> x0, blocking collectives: 18.5 us -> none
    select_n x21 -> x0, other arithmetic: 9.07 us -> none  [lap(): jnp.where(position < mine, new, old)]
    reshape x5 -> x0, local copies, waits for them, and re-layouts: 7.69 us -> none  [the longest x1 4.04 us: join(): jnp.moveaxis(array, 0, 1)]
    reduce_sum x4 -> x0, other arithmetic: 7.26 us -> none  [the longest x2 4.73 us: normalize(): jnp.mean(values * values, axis=-1, keepdims=True) + EPS]
  transfers between devices with their start and end apart: 3 -> 0, of which waited for: 1 -> 0; matrix products, arithmetic and copies ran while one was open for 11% -> 0% of each run, Pallas kernels for 0% -> 0%
where the time goes in v1:
time: 86.2 us; the launch traced here: 85.8 us
  Pallas kernels  73.9 us (86%)
  local copies, waits for them, and re-layouts  11.3 us (13%)
    pallas_call x1, Pallas kernels, body(): pl.pallas_call(functools.partial(kernel, n_sp, n_tp), out_shape=jax.Shape...  73.9 us
    unnamed x5, local copies, waits for them, and re-layouts  2.31 us

profile of v1, /device:TPU:10, one launch (start us, length us, event | category | flops | bytes accessed | tf_op | source)
XLA Modules:
  0.0 85.8 jit_solution(15086342859874757426)
XLA Ops:
  0.0 0.0 copy-start
  0.0 0.8 dynamic_slice.23
  0.8 0.7 dynamic_slice.24
  1.5 0.6 fusion.1.gates_b_ref
  2.1 1.3 %dynamic_slice.27 = f32[256]{0:T(256)} dynamic-slice(f32[1024]{0:T(1024)} %param.38, s32[]{:T(128)S(6)} %select_n.19), dynamic_slice_sizes={256} | dynamic-slice | bytes 2052 | tf_op jit(solution)/shard_map/dynamic_slice | solution.py:488
  3.4 1.3 %dynamic_slice.25 = f32[512]{0:T(512)} dynamic-slice(f32[2048]{0:T(1024)} %param.34, s32[]{:T(128)S(6)} %select_n.18), dynamic_slice_sizes={512} | dynamic-slice | bytes 4100 | tf_op jit(solution)/shard_map/dynamic_slice | solution.py:487
  4.7 0.9 %dynamic_update_slice.3.normal_ref = f32[2,256]{1,0:T(2,128)S(1)} dynamic-update-slice(f32[2,256]{1,0:T(2,128)S(1)} %broadcast_in_dim.20, f32[2,32]{1,0:T(2,128)} %param.33, s32[]{:T(128)} %constant.5.clone.1, s32[]{:T(128)S(6)} %select_n.17) | dynamic-update-slice | bytes 516 | tf_op jit(solution)/shard_map/dynamic_update_slice | solution.py:484
  5.6 0.0 copy-start.1
  5.6 0.8 constant_dynamic-slice_fusion.1
  6.5 1.3 %pad.14.extra_ref = f32[8,1024]{1,0:T(8,128)} pad(f32[2,1024]{1,0:T(2,128)} %bitcast.10, f32[]{:T(128)} %constant.10.clone.1), padding=2_4x0_0 | pad | bytes 40964 | tf_op jit(solution)/shard_map/jit(_pad)/pad | solution.py:482
  7.8 0.0 copy-done
  7.8 0.6 constant_dynamic-slice_fusion.mix_ref
  8.4 0.3 copy.24
  8.7 0.9 %pad.12.gates_w_ref = bf16[2048,128]{1,0:T(8,128)(2,1)} pad(bf16[2048,4]{1,0:T(8,128)(2,1)S(1)} %copy.24, bf16[]{:T(256)} %constant.9.clone.1), padding=0_0x0_124 | pad | bytes 540674 | tf_op jit(solution)/shard_map/jit(_pad)/pad | solution.py:475
  9.6 0.0 copy-done.1
  9.6 73.9 %shard_map.199 = bf16[256,2048]{1,0:T(8,128)(2,1)} custom-call(bf16[1024,2048]{1,0:T(8,128)(2,1)} %tokens_hbm.1, f32[1,2048]{1,0:T(1,128)} %bitcast.7, bf16[2048,512]{1,0:T(8,128)(2,1)} %wq_hbm.1, bf16[2048,512]{1,0:T(8,128)(2,1)} %wk_hbm.1, bf16[2048,512]{1,0:T(8,128)(2,1)} %wv_hbm.1, bf16[2048,512]{1,0:T(8,128)(2,1)} %wg_hbm.1, ...), custom_call_target="tpu_custom_call" | custom-call | tf_op jit(solution)/shard_map/pallas_call | solution.py:499
  83.5 2.3 %copy.27 = bf16[256,2048]{1,0:T(8,128)(2,1)} copy(bf16[256,2048]{1,0:T(8,128)(2,1)} %shard_map.199) | data formatting | bytes 2097152
  (2 shorter events, 0.0 us)
Async XLA Ops:
  0.0 7.8 %copy-start = (bf16[8,128,128]{2,1,0:T(8,128)(2,1)S(1)}, bf16[8,128,128]{2,1,0:T(8,128)(2,1)}, u32[]{:S(2)}) copy-start(bf16[8,128,128]{2,1,0:T(8,128)(2,1)} %param.37) | copy-start | bytes 786436
  5.6 4.0 %copy-start.1 = (f32[2,256]{1,0:T(2,128)}, f32[2,256]{1,0:T(2,128)S(1)}, u32[]{:S(2)}) copy-start(f32[2,256]{1,0:T(2,128)S(1)} %dynamic_update_slice.3.normal_ref) | copy-start | bytes 6148

commit v2 on v1

--- a/solution.py
+++ b/solution.py
@@ -36,8 +36,10 @@
     wk_hbm,
     wv_hbm,
     wg_hbm,
-    gates_w_ref,
-    gates_b_ref,
+    w_in_ref,
+    w_forget_ref,
+    b_in_ref,
+    b_forget_ref,
     extra_ref,
     init_ref,
     normal_ref,
@@ -86,6 +88,10 @@
     own_ref,
     link_send,
     link_recv,
+    gates_w_ref,
+    gates_b_ref,
+    raw_ref,
+    start_ref,
     local_sem,
     s_sems,
     a_sems,
@@ -147,6 +153,14 @@
 
         lax.fori_loop(0, T // size, step, 0)
 
+    heads = w_in_ref.shape[1]
+    gates_w_ref[...] = jnp.zeros_like(gates_w_ref)
+    gates_w_ref[:, 0:heads] = w_in_ref[...]
+    gates_w_ref[:, heads : 2 * heads] = w_forget_ref[...]
+    gates_b_ref[...] = jnp.zeros_like(gates_b_ref)
+    gates_b_ref[:, 0:heads] = b_in_ref[...]
+    gates_b_ref[:, heads : 2 * heads] = b_forget_ref[...]
+
     loads["tokens"].wait()
 
     def norm_tile(rows):
@@ -154,12 +168,22 @@
         scale = lax.rsqrt(jnp.mean(x * x, axis=-1, keepdims=True) + EPS)
         normed[rows, :] = (x * scale * gain_ref[...]).astype(BF16)
 
-    by_tile(norm_tile, 64)
-
-    def gate_tile(rows):
+    def early_products(t):
+        rows = pl.ds(t * TILE, TILE)
         cols_ref[rows, :] = dot(normed[rows, :], gates_w_ref[...]) + gates_b_ref[...]
-
-    by_tile(gate_tile)
+        cols_ref[rows, 2 * heads : 2 * heads + H] = extra_ref[rows, :]
+        keys = dot(normed[rows, :], wk[...])
+        for h in range(H):
+            k_ref[h, rows, :] = keys[:, h * HEAD_DIM : (h + 1) * HEAD_DIM].astype(BF16)
+
+    for t in range(tiles + 1):
+        if t == 1:
+            loads["wk"].wait()
+        if t < tiles:
+            for sub in range(0, TILE, 64):
+                norm_tile(pl.ds(t * TILE + sub, 64))
+        if t > 0:
+            early_products(t - 1)
     tri = (
         lax.broadcasted_iota(jnp.int32, (TILE, TILE), 0)
         <= lax.broadcasted_iota(jnp.int32, (TILE, TILE), 1)
@@ -168,14 +192,21 @@
     carry = jnp.zeros((8, 1), F32)
     for t in range(tiles):
         span = pl.ds(t * TILE, TILE)
-        raw = cols_ref[span, :].T[0:8]
-        log_keep = jnp.minimum(raw, 0.0) - jnp.log1p(jnp.exp(-jnp.abs(raw))) + extra_ref[:, span]
+        raw_ref[:, span] = cols_ref[span, :].T
+        own_rows = [raw_ref[pl.ds(heads + tp * H + h, 1), span] for h in range(H)]
+        added = [raw_ref[2 * heads + h : 2 * heads + h + 1, span] for h in range(H)]
+        spare = [jnp.zeros((8 - H, TILE), F32)]
+        raw = jnp.concatenate(own_rows + spare, axis=0)
+        log_keep = jnp.minimum(raw, 0.0) - jnp.log1p(jnp.exp(-jnp.abs(raw)))
+        log_keep = log_keep + jnp.concatenate(added + spare, axis=0)
         run = carry + jnp.dot(
             log_keep, tri, preferred_element_type=F32, precision=lax.Precision.HIGHEST
         )
         carry = run[:, TILE - 1 : TILE]
-        rows_ref[0:H, span] = raw[0:H] - run[H : 2 * H]
-        rows_ref[H : 2 * H, span] = run[H : 2 * H]
+        for h in range(H):
+            keep = run[h : h + 1]
+            rows_ref[h : h + 1, span] = raw_ref[pl.ds(tp * H + h, 1), span] - keep
+            rows_ref[H + h : H + h + 1, span] = keep
     for t in range(tiles):
         span = pl.ds(t * TILE, TILE)
         cols_ref[span, :] = rows_ref[:, span].T
@@ -195,7 +226,6 @@
 
         return store
 
-    project("wk", wk, heads_to(k_ref))
     project("wv", wv, heads_to(v_ref))
 
     part = HEAD_DIM // n_sp
@@ -220,7 +250,7 @@
         a_send[4 * h : 4 * h + 1, :] = jnp.broadcast_to(total + a_max, (1, HEAD_DIM))
         a_send[4 * h + 1 : 4 * h + 2, :] = jnp.broadcast_to(total, (1, HEAD_DIM))
         a_send[4 * h + 2 : 4 * h + 3, :] = normal
-        a_send[4 * h + 3 : 4 * h + 4, :] = normal_ref[h : h + 1, :]
+        a_send[4 * h + 3 : 4 * h + 4, 0:part] = normal_ref[h : h + 1, :]
 
     pl.semaphore_wait(barrier, n_sp - 1 + n_tp - 1)
     first = []
@@ -254,9 +284,9 @@
     enter_max, enter_normal = [], []
     for h in range(H):
         state = init_ref[h].astype(F32)
-        normal = jnp.zeros((1, HEAD_DIM), F32)
         for j in range(n_sp):
-            normal = normal + a_recv[j, 4 * h + 3 : 4 * h + 4, :]
+            start_ref[h : h + 1, j * part : (j + 1) * part] = a_recv[j, 4 * h + 3 : 4 * h + 4, 0:part]
+        normal = start_ref[h : h + 1, :]
         stab = jnp.zeros((1, HEAD_DIM), F32)
         my_stab, my_normal = stab, normal
         for j in range(n_sp):
@@ -327,9 +357,9 @@
             position = lax.broadcasted_iota(jnp.int32, (TILE, 1), 0) + (sp * T + t * TILE + 1)
             counts = jnp.minimum(position, window).astype(F32)
             pooled = (sums / counts - here.astype(F32)).astype(BF16)
-            mixed = dot(pooled, mix_ref[g])
+            mixed = dot(pooled, mix_ref[tp * G + g])
             pool_ref[span, lanes] = (
-                mixed * pool_gain_ref[:, lanes] * silu(pgate_ref[span, lanes])
+                mixed * pool_gain_ref[:, pl.ds(pl.multiple_of((tp * G + g) * GROUP_DIM, GROUP_DIM), GROUP_DIM)] * silu(pgate_ref[span, lanes])
             ).astype(BF16)
 
     for copy in second:
@@ -381,7 +411,7 @@
     def memory_out(rows):
         parts = []
         for h in range(H):
-            lanes = slice(h * HEAD_DIM, (h + 1) * HEAD_DIM)
+            lanes = pl.ds(pl.multiple_of((tp * H + h) * HEAD_DIM, HEAD_DIM), HEAD_DIM)
             parts.append(
                 (
                     num_ref[h, rows, :]
@@ -470,23 +500,7 @@
     PW = w_pool_input.shape[1]
     H = MW // HEAD_DIM
     G = PW // GROUP_DIM
-    sp, tp = lax.axis_index("sp"), lax.axis_index("tp")
-    cut = functools.partial(lax.dynamic_slice_in_dim, start_index=tp * H, slice_size=H)
-    gates_w = jnp.pad(
-        jnp.concatenate([cut(w_input_gate, axis=1), cut(w_forget_gate, axis=1)], axis=1),
-        ((0, 0), (0, 128 - 2 * H)),
-    )
-    gates_b = jnp.pad(
-        jnp.concatenate([cut(input_bias, axis=0), cut(forget_bias, axis=0)]), (0, 128 - 2 * H)
-    )[None]
-    extra = jnp.pad(forget_extra.T, ((H, 8 - 2 * H), (0, 0)))
     part = initial_normal.shape[1]
-    normal = lax.dynamic_update_slice(
-        jnp.zeros((H, HEAD_DIM), F32), initial_normal, (0, sp * part)
-    )
-    mem_gain = lax.dynamic_slice_in_dim(memory_gain, tp * MW, MW, 0)[None]
-    gain_pool = lax.dynamic_slice_in_dim(pool_gain, tp * PW, PW, 0)[None]
-    mix = lax.dynamic_slice_in_dim(pool_mix, tp * G, G, 0)
     wire = BF16 if part % 16 == 0 else F32
     chips = n_tp // 2
     block = T // n_tp
@@ -499,7 +513,7 @@
     return pl.pallas_call(
         functools.partial(kernel, n_sp, n_tp),
         out_shape=jax.ShapeDtypeStruct((block, D), BF16),
-        in_specs=[hbm, vmem, hbm, hbm, hbm, hbm, vmem, vmem, vmem, vmem, vmem, vmem]
+        in_specs=[hbm, vmem, hbm, hbm, hbm, hbm, vmem, vmem, vmem, vmem, vmem, vmem, vmem, vmem]
         + [hbm, hbm, vmem, vmem, hbm, hbm, vmem],
         out_specs=vmem,
         scratch_shapes=[
@@ -539,6 +553,10 @@
             V((slots, size, D), BF16),
             V((slots, size, D), BF16),
             V((slots, size, D), BF16),
+            V((D, 128), BF16),
+            V((1, 128), F32),
+            V((128, T), F32),
+            V((8, HEAD_DIM), F32),
             dma((9,)),
             dma((2, n_sp)),
             dma((2, n_sp)),
@@ -558,16 +576,18 @@
         w_key,
         w_value,
         memory_output_gate_weight,
-        gates_w,
-        gates_b,
-        extra,
+        w_input_gate,
+        w_forget_gate,
+        input_bias[None],
+        forget_bias[None],
+        forget_extra,
         initial_memory,
-        normal,
-        mem_gain,
+        initial_normal,
+        memory_gain[None],
         w_pool_input,
         w_pool_gate,
-        mix,
-        gain_pool,
+        pool_mix,
+        pool_gain[None],
         w_out_memory,
         w_out_pool,
         post_gain[None],

time: 86.2 us -> 79.5 us (0.922)
  local copies, waits for them, and re-layouts: 11.3 us -> 7.58 us
  Pallas kernels: 73.9 us -> 71.6 us
    dynamic_slice x6 -> x0, local copies, waits for them, and re-layouts: 5.58 us -> none  [the longest x1 1.33 us: body(): gain_pool = lax.dynamic_slice_in_dim(pool_gain, tp * PW, PW, 0)[None]]
    unnamed x5 -> x4, local copies, waits for them, and re-layouts: 2.31 us -> 7.58 us
    pallas_call x1, Pallas kernels: 73.9 us -> 71.6 us  [body(): pl.pallas_call(functools.partial(kernel, n_sp, n_tp), out_shape=jax.Shape...]
    pad x2 -> x0, local copies, waits for them, and re-layouts: 2.23 us -> none  [the longest x1 1.32 us: body(): extra = jnp.pad(forget_extra.T, ((H, 8 - 2 * H), (0, 0)))]
    dynamic_update_slice x1 -> x0, local copies, waits for them, and re-layouts: 0.87 us -> none  [body(): lax.dynamic_update_slice(jnp.zeros((H, HEAD_DIM), F32), initial_normal, (...]
where the time goes in v2:
time: 79.5 us; the launch traced here: 79.2 us
  Pallas kernels  71.6 us (90%)
  local copies, waits for them, and re-layouts  7.58 us (10%)
    pallas_call x1, Pallas kernels, body(): pl.pallas_call(functools.partial(kernel, n_sp, n_tp), out_shape=jax.Shape...  71.6 us
    unnamed x4, local copies, waits for them, and re-layouts  7.58 us

profile of v2, /device:TPU:10, one launch (start us, length us, event | category | flops | bytes accessed | tf_op | source)
XLA Modules:
  0.0 79.2 jit_solution(615997900403185305)
XLA Ops:
  0.0 1.8 %copy.22.w_in_ref = bf16[2048,8]{1,0:T(8,128)(2,1)} copy(bf16[2048,8]{0,1:T(8,128)(2,1)} %param.27) | data formatting | bytes 65536 | tf_op args[6]
  1.8 1.8 %copy.23.w_forget_ref = bf16[2048,8]{1,0:T(8,128)(2,1)} copy(bf16[2048,8]{0,1:T(8,128)(2,1)} %param.28) | data formatting | bytes 65536 | tf_op args[7]
  3.5 1.7 %copy.24.extra_ref = f32[1024,2]{1,0:T(8,128)} copy(f32[1024,2]{0,1:T(2,128)} %param.31) | data formatting | bytes 16384 | tf_op args[10]
  5.3 71.6 %shard_map.199 = bf16[256,2048]{1,0:T(8,128)(2,1)} custom-call(bf16[1024,2048]{1,0:T(8,128)(2,1)} %tokens_hbm.1, f32[1,2048]{1,0:T(1,128)} %bitcast.6, bf16[2048,512]{1,0:T(8,128)(2,1)} %wq_hbm.1, bf16[2048,512]{1,0:T(8,128)(2,1)} %wk_hbm.1, bf16[2048,512]{1,0:T(8,128)(2,1)} %wv_hbm.1, bf16[2048,512]{1,0:T(8,128)(2,1)} %wg_hbm.1, ...), custom_call_target="tpu_custom_call" | custom-call | tf_op jit(solution)/shard_map/pallas_call | solution.py:513
  76.9 2.3 %copy.26 = bf16[256,2048]{1,0:T(8,128)(2,1)} copy(bf16[256,2048]{1,0:T(8,128)(2,1)} %shard_map.199) | data formatting | bytes 2097152
